TPU v7x, 32 devices: a whole 2x2x4 slice. The times are simulated.
32 devices in a mesh: sp: 16 (over z, y, x), tp: 2 (over core).
Axes of the slice: x: 2, y: 2, z: 4, core: 2. Of those that a mesh axis runs over, the one named last changes fastest.
Arguments:
- residual: bfloat16 [2048, 4096], P('tp', 'sp'), may hold values from -6 to 6
- values: bfloat16 [4096, 4096], P('sp', 'tp'), may hold values from -6 to 6
- gate_input: bfloat16 [4096, 4096], P('sp', 'tp'), may hold values from -6 to 6
- group_keys: bfloat16 [4096, 3072], P('sp', 'tp'), may hold values from -6 to 6
- time_step: float32 [64, 4096], P('tp', 'sp'), may hold values from -8 to 14
- decay_rate: float32 [64], P('tp'), may hold values from 0 to 2
- skip_gain: float32 [64], P('tp'), may hold values from 0.25 to 2
- conv_values: bfloat16 [4, 4096], P(None, 'tp'), may hold values from -3 to 3
- conv_keys: bfloat16 [4, 3072], P(None, 'tp'), may hold values from -3 to 3
- mix_gain: float32 [4096], P('tp'), may hold values from 0.1 to 1.9
- out_weight: bfloat16 [4096, 2048], P('tp'), may hold values from -0.09375 to 0.09375
- norm_gain: float32 [2048], replicated, may hold values from 0.1 to 1.9
- hidden_gate: bfloat16 [2048, 5120], P('sp', 'tp'), may hold values from -0.125 to 0.125
- hidden_up: bfloat16 [2048, 5120], P('sp', 'tp'), may hold values from -0.125 to 0.125
- hidden_conv: bfloat16 [2, 3, 5120], P(None, None, 'tp'), may hold values from -3.5 to 3.5
- hidden_down: bfloat16 [5120, 2048], P('tp', 'sp'), may hold values from -0.078125 to 0.078125
Outputs:
- layer_out: bfloat16 [2048, 4096], P('tp', 'sp')
All inputs are finite; a program needn't handle non-finite values.
Results may differ from a plain program's by a relative error of at most 0.019.
Values may be sent and summed in bfloat16 or wider, within the bound.
A program may use at most 128 MiB of HBM per device.

v0:
```python
import jax
import jax.numpy as jnp
from jax import lax
from jax.sharding import PartitionSpec as P

GROUP_HEADS = 8
HEAD_SIZE = 64
STATE_WIDE = 128
STATE_NARROW = 64
BLOCK = 128
NORM_FLOOR = 0.1
HIGHEST = lax.Precision.HIGHEST


def from_behind(value, axis, steps):
    count = lax.axis_size(axis)
    first, last = (max(0, -steps), min(count, count - steps))
    return lax.ppermute(value, axis, [(source, source + steps) for source in range(first, last)])


def prefix(shard, axis, join, neutral):
    place = lax.axis_index(axis)
    gathered = jax.tree.map(
        lambda a, kind: lax.all_gather(a.astype(kind), axis),
        shard,
        (jnp.bfloat16, jnp.bfloat16, jnp.bfloat16, jnp.bfloat16),
    )
    state = jax.tree.map(lambda a, e: jnp.zeros_like(a) + jnp.asarray(e, a.dtype), shard, neutral)

    def one(lap, state):
        return join(
            state,
            jax.tree.map(
                lambda a, own: lax.dynamic_index_in_dim(a, lap, 0, False).astype(own.dtype),
                gathered,
                shard,
            ),
        )

    return lax.fori_loop(0, place, one, state)


def from_partner_2(shard, axis, stride):
    return lax.ppermute(shard, axis, [(i, i ^ 1 << stride) for i in range(lax.axis_size(axis))])


def tap_sum(joined, weights, row_count):
    summed = weights[0].astype(jnp.float32) * joined[0:row_count]
    for tap_index in range(1, weights.shape[0]):
        summed = (
            summed
            + weights[tap_index].astype(jnp.float32) * joined[tap_index : tap_index + row_count]
        )
    return summed


def block_heads(inputs, in_keys, out_keys, deltas, decay_rates, skip_table, carried):
    length = inputs.shape[0]
    running = jnp.cumsum(-decay_rates * deltas, axis=0)
    weighted = inputs * deltas[..., None]
    scores = jnp.einsum("ign,jgn->gij", out_keys, in_keys, precision=HIGHEST)
    by_head = jnp.transpose(running, (1, 2, 0))
    between = by_head[..., :, None] - by_head[..., None, :]
    lower_mask = jnp.tril(jnp.ones((length, length), dtype=bool))
    decays = jnp.exp(jnp.where(lower_mask, between, -jnp.inf))
    inside = jnp.einsum("ghij,jghp->ighp", scores[:, None] * decays, weighted, precision=HIGHEST)
    carried_part = (
        jnp.einsum("ign,ghpn->ighp", out_keys, carried, precision=HIGHEST)
        * jnp.exp(running)[..., None]
    )
    to_end = jnp.exp(by_head[..., -1:] - by_head)
    fresh_state = jnp.einsum("jgn,ghj,jghp->ghpn", in_keys, to_end, weighted, precision=HIGHEST)
    updated = carried * jnp.exp(by_head[..., -1])[..., None, None] + fresh_state
    return (inside + carried_part + inputs * skip_table[..., None], updated)


def contract_rows(left, right):
    return lax.dot_general(
        left, right, (((0,), (0,)), ((), ())), preferred_element_type=jnp.float32
    )


def combine_states(first_part, second_part):
    return (
        first_part[0] * second_part[0],
        first_part[1] * second_part[0][..., None, None] + second_part[1],
        first_part[2] * second_part[2],
        first_part[3] * second_part[2][..., None, None] + second_part[3],
    )


def hidden_taps(both_pre, edge_cols, taps, row_count):
    joined_hidden = jnp.concatenate([edge_cols, both_pre], axis=2).astype(jnp.float32)
    conv_total = taps[:, 0, :, None].astype(jnp.float32) * joined_hidden[:, :, 0:row_count]
    for tap_index in range(1, taps.shape[1]):
        conv_total = (
            conv_total
            + taps[:, tap_index, :, None].astype(jnp.float32)
            * joined_hidden[:, :, tap_index : tap_index + row_count]
        )
    return (jax.nn.silu(conv_total[0]) * conv_total[1]).astype(jnp.bfloat16)


def local(
    residual,
    values,
    gate_input,
    group_keys,
    time_step,
    decay_rate,
    skip_gain,
    conv_values,
    conv_keys,
    mix_gain,
    out_weight,
    norm_gain,
    hidden_gate,
    hidden_up,
    hidden_conv,
    hidden_down,
):
    row_count = values.shape[0]
    value_cols = values.shape[1]
    tap_count = conv_values.shape[0]
    tail_rows = jnp.concatenate(
        [values[row_count - tap_count + 1 :], group_keys[row_count - tap_count + 1 :]], axis=1
    )
    before_rows = from_behind(tail_rows, "sp", 1)
    joined_values = jnp.concatenate([before_rows[:, :value_cols], values], axis=0).astype(
        jnp.float32
    )
    joined_keys = jnp.concatenate([before_rows[:, value_cols:], group_keys], axis=0).astype(
        jnp.float32
    )
    group_count = group_keys.shape[1] // (2 * STATE_WIDE + 2 * STATE_NARROW)
    inputs = jax.nn.silu(tap_sum(joined_values, conv_values, row_count)).reshape(
        row_count, group_count, GROUP_HEADS, HEAD_SIZE
    )
    key_rows = jax.nn.silu(tap_sum(joined_keys, conv_keys, row_count)).reshape(
        row_count, group_count, -1
    )
    deltas = jax.nn.softplus(time_step).T.reshape(row_count, group_count, GROUP_HEADS)
    rate_table = decay_rate.reshape(group_count, GROUP_HEADS)
    skip_table = skip_gain.reshape(group_count, GROUP_HEADS)
    running = jnp.cumsum(-rate_table * deltas, axis=0)
    half_heads = GROUP_HEADS // 2
    wide_end = 2 * STATE_WIDE

    def run_kind(head_first, head_last, key_first, state_width):
        in_keys = key_rows[..., key_first : key_first + state_width]
        out_keys = key_rows[..., key_first + state_width : key_first + 2 * state_width]
        carried = jnp.zeros(
            (group_count, head_last - head_first, HEAD_SIZE, state_width), jnp.float32
        )
        block_outs = []
        for block_index in range(row_count // BLOCK):
            row_first = block_index * BLOCK
            row_last = row_first + BLOCK
            block_out, carried = block_heads(
                inputs[row_first:row_last, :, head_first:head_last],
                in_keys[row_first:row_last],
                out_keys[row_first:row_last],
                deltas[row_first:row_last, :, head_first:head_last],
                rate_table[:, head_first:head_last],
                skip_table[:, head_first:head_last],
                carried,
            )
            block_outs.append(block_out)
        return (jnp.concatenate(block_outs, axis=0), carried, out_keys)

    wide_local, wide_state, wide_keys = run_kind(0, half_heads, 0, STATE_WIDE)
    narrow_local, narrow_state, narrow_keys = run_kind(
        half_heads, GROUP_HEADS, wide_end, STATE_NARROW
    )
    span_decay = jnp.exp(running[-1])
    start_value = (
        jnp.ones_like(span_decay[:, :half_heads]),
        jnp.zeros_like(wide_state),
        jnp.ones_like(span_decay[:, half_heads:]),
        jnp.zeros_like(narrow_state),
    )
    incoming = prefix(
        (span_decay[:, :half_heads], wide_state, span_decay[:, half_heads:], narrow_state),
        "sp",
        combine_states,
        start_value,
    )
    growth = jnp.exp(running)[..., None]
    wide_out = (
        wide_local
        + jnp.einsum("ign,ghpn->ighp", wide_keys, incoming[1], precision=HIGHEST)
        * growth[:, :, :half_heads]
    )
    narrow_out = (
        narrow_local
        + jnp.einsum("ign,ghpn->ighp", narrow_keys, incoming[3], precision=HIGHEST)
        * growth[:, :, half_heads:]
    )
    mixer_out = jnp.concatenate([wide_out, narrow_out], axis=2).reshape(row_count, value_cols)
    gated_out = mixer_out * jax.nn.silu(gate_input.astype(jnp.float32))
    squares = lax.psum(jnp.sum(gated_out * gated_out, axis=1), "tp")
    inverse_rms = lax.rsqrt(squares / (value_cols * lax.axis_size("tp")) + NORM_FLOOR)
    normed = (gated_out * inverse_rms[:, None] * mix_gain).astype(jnp.bfloat16)
    mixer_sum = lax.psum_scatter(
        lax.dot_general(
            out_weight, normed, (((0,), (1,)), ((), ())), preferred_element_type=jnp.float32
        ).astype(jnp.bfloat16),
        "tp",
        scatter_dimension=0,
        tiled=True,
    ).astype(jnp.float32)
    own_merged = (residual.astype(jnp.float32) + mixer_sum).astype(jnp.bfloat16)
    merged = lax.all_gather(own_merged, "tp", axis=0, tiled=True)
    merged_wide = merged.astype(jnp.float32)
    inverse_norm = lax.rsqrt(jnp.mean(merged_wide * merged_wide, axis=0) + NORM_FLOOR)
    lifted = (merged_wide * inverse_norm[None, :] * norm_gain[:, None]).astype(jnp.bfloat16)
    hidden_cols = hidden_gate.shape[1]
    edge_taps = hidden_conv.shape[1]
    half_cols = hidden_cols // 2
    parity = lax.axis_index("sp") % 2
    first_member = parity == 0
    sp_count = lax.axis_size("sp")
    weight_rows = hidden_gate.shape[0]
    gate_tiles = jnp.tile(
        jnp.stack([hidden_gate[:, :half_cols], hidden_gate[:, half_cols:]]), (sp_count // 2, 1, 1)
    )
    up_tiles = jnp.tile(
        jnp.stack([hidden_up[:, :half_cols], hidden_up[:, half_cols:]]), (sp_count // 2, 1, 1)
    )
    gate_half, up_half = (
        lax.all_to_all(gate_tiles, "sp", split_axis=0, concat_axis=0, tiled=True),
        lax.all_to_all(up_tiles, "sp", split_axis=0, concat_axis=0, tiled=True),
    )
    gate_half = gate_half.reshape(sp_count * weight_rows, half_cols)
    up_half = up_half.reshape(sp_count * weight_rows, half_cols)
    partner_lifted = from_partner_2(lifted, "sp", 0)
    pair_lifted = jnp.where(
        first_member,
        jnp.concatenate([lifted, partner_lifted], axis=1),
        jnp.concatenate([partner_lifted, lifted], axis=1),
    )
    pair_count = 2 * row_count
    pair_pre = jnp.stack(
        [contract_rows(gate_half, pair_lifted), contract_rows(up_half, pair_lifted)]
    ).astype(jnp.bfloat16)
    pair_edge = from_behind(pair_pre[:, :, pair_count - edge_taps + 1 :], "sp", 2)
    half_taps = lax.dynamic_slice_in_dim(hidden_conv, parity * half_cols, half_cols, 2)
    half_hidden = hidden_taps(pair_pre, pair_edge, half_taps, pair_count)
    own_part = lax.dynamic_slice_in_dim(half_hidden, parity * row_count, row_count, 1)
    for_partner = lax.dynamic_slice_in_dim(half_hidden, (1 - parity) * row_count, row_count, 1)
    from_partner = from_partner_2(for_partner, "sp", 0)
    hidden = jnp.where(
        first_member,
        jnp.concatenate([own_part, from_partner], axis=0),
        jnp.concatenate([from_partner, own_part], axis=0),
    )
    down_whole = lax.all_gather(hidden_down, "sp", axis=1, tiled=True)
    hidden_sum = lax.psum_scatter(
        contract_rows(down_whole, hidden).astype(jnp.bfloat16),
        "tp",
        scatter_dimension=0,
        tiled=True,
    ).astype(jnp.float32)
    return (own_merged.astype(jnp.float32) + hidden_sum).astype(jnp.bfloat16)


def solution(mesh):
    in_specs = (
        P("tp", "sp"),
        P("sp", "tp"),
        P("sp", "tp"),
        P("sp", "tp"),
        P("tp", "sp"),
        P("tp"),
        P("tp"),
        P(None, "tp"),
        P(None, "tp"),
        P("tp"),
        P("tp", None),
        P(),
        P("sp", "tp"),
        P("sp", "tp"),
        P(None, None, "tp"),
        P("tp", "sp"),
    )
    out_specs = P("tp", "sp")
    return jax.shard_map(local, mesh=mesh, in_specs=in_specs, out_specs=out_specs, check_vma=False)
```

profile of v0, /device:TPU:0, one launch (start us, length us, event | category | flops | bytes accessed | tf_op | source)
XLA Modules:
  0.0 622.7 jit_solution(8149238865578526616)
XLA Ops:
  8.2 4.9 collective-permute-start
  22.5 2.4 divide_multiply_fusion.1
  30.2 2.5 fusion.43
  33.9 2.8 tile.8
  36.6 6.0 all-to-all-start
  52.9 125.0 %all-gather.4 = bf16[16,4,4]{2,1,0:T(4,128)(2,1)S(1)} all-gather(bf16[1,4,4]{2,1,0:T(4,128)(2,1)S(1)} %get-tuple-element.151), channel_id=2, replica_groups=mesh['sp'=16,'tp'=2] {'sp'}, dimensions={0}, use_global_device_ids=true | all-gather | bytes 544 | tf_op jit(solution)/shard_map/all_gather | solution.py:24
  177.9 77.3 %all-gather.5 = bf16[16,4,4]{2,1,0:T(4,128)(2,1)S(1)} all-gather(bf16[1,4,4]{2,1,0:T(4,128)(2,1)S(1)} %get-tuple-element.150), channel_id=4, replica_groups=mesh['sp'=16,'tp'=2] {'sp'}, dimensions={0}, use_global_device_ids=true | all-gather | bytes 544 | tf_op jit(solution)/shard_map/all_gather | solution.py:24
  262.3 3.0 fusion.38
  265.3 2.9 fusion.32
  268.3 3.0 fusion.34
  279.2 2.5 psum.7
  281.7 7.0 %fusion.6 = bf16[2048,256]{0,1:T(8,128)(2,1)} fusion(bf16[2048,2048]{1,0:T(8,128)(2,1)} %param.28, f32[2048]{0:T(1024)S(1)} %copy-done.19, f32[256]{0:T(256)S(1)} %add_rsqrt_fusion.1, f32[256,2048]{1,0:T(8,128)S(1)} %copy.153, bf16[256,2048]{1,0:T(8,128)(2,1)S(1)} %copy-done.5), kind=kOutput, calls=%fused_computation.24 | convolution fusion | flops 2152726528 | bytes 12592128 | tf_op jit(solution)/shard_map/dot_general | solution.py:205
  290.1 36.7 %reduce-scatter.3.cloned.1.call-done = bf16[1024,256]{0,1:T(8,128)(2,1)} async-done(((bf16[2048,256]{0,1:T(8,128)(2,1)}), bf16[1024,256]{0,1:T(8,128)(2,1)}) %reduce-scatter.3.cloned.1.call-update) | async-done | bytes 524304 | tf_op jit(solution)/shard_map/reduce_scatter | solution.py:204
  329.6 2.8 tile.20
  332.4 6.9 %all-to-all-start.1 = ((bf16[16,128,1280]{2,1,0:T(8,128)(2,1)}), bf16[16,128,1280]{2,1,0:T(8,128)(2,1)}, u32[]{:S(2)}, u32[]{:S(2)}) async-start(bf16[16,128,1280]{2,1,0:T(8,128)(2,1)} %bitcast.260), calls=%async_computation.2 | async-start | bytes 10485760 | tf_op jit(solution)/shard_map/all_to_all | solution.py:232
  344.5 55.0 %collective-permute-done.1 = bf16[2048,256]{0,1:T(8,128)(2,1)S(1)} collective-permute-done((bf16[2048,256]{0,1:T(8,128)(2,1)S(1)}, bf16[2048,256]{0,1:T(8,128)(2,1)S(1)}, u32[]{:S(2)}, u32[]{:S(2)}) %collective-permute-start.1) | collective-permute-done | bytes 1048608 | tf_op jit(solution)/shard_map/ppermute | solution.py:44
  399.5 5.7 fusion.2
  405.2 75.9 %all-to-all-done.1 = bf16[16,128,1280]{2,1,0:T(8,128)(2,1)} async-done(((bf16[16,128,1280]{2,1,0:T(8,128)(2,1)}), bf16[16,128,1280]{2,1,0:T(8,128)(2,1)}, u32[]{:S(2)}, u32[]{:S(2)}) %all-to-all-start.1) | async-done | bytes 5242912 | tf_op jit(solution)/shard_map/all_to_all | solution.py:232
  481.1 6.7 %fusion.3 = bf16[1,1280,512]{1,2,0:T(8,128)(2,1)S(1)} fusion(bf16[2048,1280]{1,0:T(8,128)(2,1)} %bitcast.75, bf16[2048,256]{0,1:T(8,128)(2,1)} %copy-done.18, bf16[2048,256]{0,1:T(8,128)(2,1)} %copy-done.7, pred[]{:T(512)S(6)} %eq.5), kind=kOutput, calls=%fused_computation.12 | convolution fusion | flops 2694447104 | bytes 8650753 | tf_op jit(solution)/shard_map/dot_general | solution.py:78
  487.8 10.7 %collective-permute-start.2 = (bf16[2,1280,2]{1,2,0:T(2,128)(2,1)S(1)}, bf16[2,1280,2]{1,2,0:T(2,128)(2,1)S(1)}, u32[]{:S(2)}, u32[]{:S(2)}) collective-permute-start(bf16[2,1280,2]{1,2,0:T(2,128)(2,1)S(1)} %pad_maximum_fusion.4), channel_id=1, source_target_pairs={{0,4},{2,6},{4,8},{6,10},{8,12},{10,14},{12,16},{14,18},{16,20},{1... | collective-permute-start | bytes 30728 | tf_op jit(solution)/shard_map/ppermute | solution.py:18
  502.8 30.5 %collective-permute-done.3 = bf16[1280,256]{0,1:T(8,128)(2,1)S(1)} collective-permute-done((bf16[1280,256]{0,1:T(8,128)(2,1)S(1)}, bf16[1280,256]{0,1:T(8,128)(2,1)S(1)}, u32[]{:S(2)}, u32[]{:S(2)}) %collective-permute-start.3) | collective-permute-done | bytes 655392 | tf_op jit(solution)/shard_map/ppermute | solution.py:44
  533.3 59.3 %all-gather.13.cloned.1.call-done = bf16[2560,2048]{1,0:T(8,128)(2,1)} async-done(((bf16[2560,128]{1,0:T(8,128)(2,1)}), bf16[2560,2048]{1,0:T(8,128)(2,1)}) %all-gather.13.cloned.1.call-update) | async-done | bytes 10485776 | tf_op jit(solution)/shard_map/all_gather | solution.py:257
  592.6 7.9 %fusion.7 = bf16[2048,256]{0,1:T(8,128)(2,1)} fusion(bf16[2560,2048]{1,0:T(8,128)(2,1)} %all-gather.13.cloned.1.call-done, bf16[1280,256]{0,1:T(8,128)(2,1)S(1)} %collective-permute-done.3, bf16[1280,256]{0,1:T(8,128)(2,1)S(1)} %get-tuple-element.121, pred[]{:T(512)S(6)} %eq.5), kind=kOutput, calls=%fused_computation.25 | convolution fusion | flops 2690777088 | bytes 12845057 | tf_op jit(solution)/shard_map/dot_general | solution.py:78
  600.5 12.9 %reduce-scatter.5.cloned.1.call-done = bf16[1024,256]{0,1:T(8,128)(2,1)} async-done(((bf16[2048,256]{0,1:T(8,128)(2,1)}), bf16[1024,256]{0,1:T(8,128)(2,1)}) %reduce-scatter.5.cloned.1.call-update) | async-done | bytes 524304 | tf_op jit(solution)/shard_map/reduce_scatter | solution.py:258
  (165 shorter events, 58.0 us)
Async XLA Ops:
  6.5 9.2 %copy-start.8 = (bf16[256,1536]{1,0:T(8,128)(2,1)S(1)}, bf16[256,1536]{1,0:T(8,128)(2,1)}, u32[]{:S(2)}) copy-start(bf16[256,1536]{1,0:T(8,128)(2,1)} %param.21) | copy-start | bytes 2359300
  6.5 9.0 %copy-start.13 = (bf16[4,2048]{1,0:T(4,128)(2,1)S(1)}, bf16[4,2048]{1,0:T(4,128)(2,1)}, u32[]{:S(2)}) copy-start(bf16[4,2048]{1,0:T(4,128)(2,1)} %param.25) | copy-start | bytes 49156
  6.5 9.1 %copy-start.14 = (bf16[4,1536]{1,0:T(4,128)(2,1)S(1)}, bf16[4,1536]{1,0:T(4,128)(2,1)}, u32[]{:S(2)}) copy-start(bf16[4,1536]{1,0:T(4,128)(2,1)} %param.26) | copy-start | bytes 36868
  6.5 264.8 %all-gather.17.cloned.1.call-start = ((), (), s32[]{:S(2)}) async-start(), calls=%async_computation.9 | async-start | bytes 4456448 | tf_op jit(solution)/shard_map/all_gather | solution.py:24
  8.2 8.9 %collective-permute-start = (bf16[3,3584]{1,0:T(4,128)(2,1)S(1)}, bf16[3,3584]{1,0:T(4,128)(2,1)S(1)}, u32[]{:S(2)}, u32[]{:S(2)}) collective-permute-start(bf16[3,3584]{1,0:T(4,128)(2,1)S(1)} %pad_maximum_fusion.3), channel_id=1, source_target_pairs={{0,2},{2,4},{4,6},{6,8},{8,10},{10,12},{12,14},{14,16},{16,18},{18... | collective-permute-start | bytes 64520 | tf_op jit(solution)/shard_map/ppermute | solution.py:18
  26.9 244.4 %all-gather.15.cloned.1.call-start = ((), (), s32[]{:S(2)}) async-start(), calls=%async_computation.8 | async-start | bytes 4456448 | tf_op jit(solution)/shard_map/all_gather | solution.py:24
  36.6 292.9 %all-to-all-start = ((bf16[16,128,1280]{2,1,0:T(8,128)(2,1)}), bf16[16,128,1280]{2,1,0:T(8,128)(2,1)}, u32[]{:S(2)}, u32[]{:S(2)}) async-start(bf16[16,128,1280]{2,1,0:T(8,128)(2,1)} %bitcast.259), calls=%async_computation.1 | async-start | bytes 10485760 | tf_op jit(solution)/shard_map/all_to_all | solution.py:231
  42.6 4.9 copy-start.12
  42.6 8.5 %copy-start.17 = (f32[32]{0:T(128)S(1)}, f32[32]{0:T(128)}, u32[]{:S(2)}) copy-start(f32[32]{0:T(128)} %param.24) | copy-start | bytes 388
  42.7 284.1 %reduce-scatter.3.cloned.1.call-start = ((), (), s32[]{:S(2)}) async-start(), calls=%async_computation.4 | async-start | bytes 1572864 | tf_op jit(solution)/shard_map/reduce_scatter | solution.py:204
  46.4 4.8 copy-start.6
  288.7 40.7 %copy-start.9 = (bf16[128,2560]{1,0:T(8,128)(2,1)S(1)}, bf16[128,2560]{1,0:T(8,128)(2,1)}, u32[]{:S(2)}) copy-start(bf16[128,2560]{1,0:T(8,128)(2,1)} %param.31) | copy-start | bytes 1966084
  288.7 50.7 %all-gather.11.cloned.1.call-start = ((), (), s32[]{:S(2)}) async-start(), calls=%async_computation.5 | async-start | bytes 1572864 | tf_op jit(solution)/shard_map/all_gather | solution.py:213
  328.9 263.7 %all-gather.13.cloned.1.call-start = ((), (), s32[]{:S(2)}) async-start(), calls=%async_computation.6 | async-start | bytes 11141120 | tf_op jit(solution)/shard_map/all_gather | solution.py:257
  332.4 8.6 %copy-start.15 = (f32[2048]{0:T(1024)S(1)}, f32[2048]{0:T(1024)}, u32[]{:S(2)}) copy-start(f32[2048]{0:T(1024)} %param.29) | copy-start | bytes 24580
  332.4 148.7 %all-to-all-start.1 = ((bf16[16,128,1280]{2,1,0:T(8,128)(2,1)}), bf16[16,128,1280]{2,1,0:T(8,128)(2,1)}, u32[]{:S(2)}, u32[]{:S(2)}) async-start(bf16[16,128,1280]{2,1,0:T(8,128)(2,1)} %bitcast.260), calls=%async_computation.2 | async-start | bytes 10485760 | tf_op jit(solution)/shard_map/all_to_all | solution.py:232
  339.4 274.0 %reduce-scatter.5.cloned.1.call-start = ((), (), s32[]{:S(2)}) async-start(), calls=%async_computation.7 | async-start | bytes 1572864 | tf_op jit(solution)/shard_map/reduce_scatter | solution.py:258
  342.5 62.7 %copy-start.7 = (bf16[2048,256]{0,1:T(8,128)(2,1)}, bf16[2048,256]{0,1:T(8,128)(2,1)S(1)}, u32[]{:S(2)}) copy-start(bf16[2048,256]{0,1:T(8,128)(2,1)S(1)} %fusion.14) | copy-start | bytes 3145732
  342.5 56.9 %collective-permute-start.1 = (bf16[2048,256]{0,1:T(8,128)(2,1)S(1)}, bf16[2048,256]{0,1:T(8,128)(2,1)S(1)}, u32[]{:S(2)}, u32[]{:S(2)}) collective-permute-start(bf16[2048,256]{0,1:T(8,128)(2,1)S(1)} %fusion.14), channel_id=1, source_target_pairs={{0,2},{2,0},{4,6},{6,4},{8,10},{10,8},{12,14},{14,12},{16,18},{18,... | collective-permute-start | bytes 3145736 | tf_op jit(solution)/shard_map/ppermute | solution.py:44
  399.5 5.8 copy-start.18
  487.8 10.8 %copy-start.16 = (bf16[2,3,2560]{2,0,1:T(2,128)(2,1)S(1)}, bf16[2,3,2560]{2,0,1:T(2,128)(2,1)}, u32[]{:S(2)}) copy-start(bf16[2,3,2560]{2,0,1:T(2,128)(2,1)} %param.32) | copy-start | bytes 92164
  487.8 11.9 %collective-permute-start.2 = (bf16[2,1280,2]{1,2,0:T(2,128)(2,1)S(1)}, bf16[2,1280,2]{1,2,0:T(2,128)(2,1)S(1)}, u32[]{:S(2)}, u32[]{:S(2)}) collective-permute-start(bf16[2,1280,2]{1,2,0:T(2,128)(2,1)S(1)} %pad_maximum_fusion.4), channel_id=1, source_target_pairs={{0,4},{2,6},{4,8},{6,10},{8,12},{10,14},{12,16},{14,18},{16,20},{1... | collective-permute-start | bytes 30728 | tf_op jit(solution)/shard_map/ppermute | solution.py:18
  502.7 30.6 %collective-permute-start.3 = (bf16[1280,256]{0,1:T(8,128)(2,1)S(1)}, bf16[1280,256]{0,1:T(8,128)(2,1)S(1)}, u32[]{:S(2)}, u32[]{:S(2)}) collective-permute-start(bf16[1280,256]{0,1:T(8,128)(2,1)S(1)} %get-tuple-element.122), channel_id=1, source_target_pairs={{0,2},{2,0},{4,6},{6,4},{8,10},{10,8},{12,14},{14,12},{16,18},{18,... | collective-permute-start | bytes 1966088 | tf_op jit(solution)/shard_map/ppermute | solution.py:44
  592.6 20.9 %copy-start.2 = (bf16[1024,256]{0,1:T(8,128)(2,1)S(1)}, bf16[1024,256]{0,1:T(8,128)(2,1)}, u32[]{:S(2)}) copy-start(bf16[1024,256]{0,1:T(8,128)(2,1)} %add_convert_fusion.1) | copy-start | bytes 1572868
  (8 other events, 17.3 us)
Sparse Core Ops, SparseCore 0:
  27.0 157.4 all-gather.16
  187.2 74.3 all-gather.14
  288.8 37.9 reduce-scatter.2
  329.0 10.1 all-gather.10
  341.7 250.7 all-gather.12
  600.6 12.7 reduce-scatter.4
where the time goes:
time: 632 us; the launch traced here: 623 us
  waiting for transfers between devices  272 us (43%)
  blocking collectives  205 us (32%)
  matrix products  52.4 us (8%)
  starting transfers between devices  30.7 us (5%)
  local copies, waits for them, and re-layouts  26.2 us (4%)
  other arithmetic  21.9 us (3%)
  between operations  14.4 us (2%)
    all_gather x2, blocking collectives, prefix(): lax.all_gather(a.astype(kind), axis)  202 us
    ppermute x2, waiting for transfers between devices, from_partner_2(): lax.ppermute(shard, axis, [(i, i ^ 1 << stride) for i in range(lax.axis_s...  85.5 us
    all_to_all x1, waiting for transfers between devices, local(): lax.all_to_all(up_tiles, 'sp', split_axis=0, concat_axis=0, tiled=True)  75.9 us
    all_gather x1, waiting for transfers between devices, local(): down_whole = lax.all_gather(hidden_down, 'sp', axis=1, tiled=True)  59.3 us
    reduce_scatter x1, waiting for transfers between devices, local(): lax.psum_scatter(lax.dot_general(out_weight, normed, (((0,), (1,)), ((),...  36.7 us
    dot_general x3, matrix products, contract_rows(): lax.dot_general(left, right, (((0,), (0,)), ((), ())), preferred_element_...  20.3 us
    ppermute x2, starting transfers between devices, from_behind(): lax.ppermute(value, axis, [(source, source + steps) for source in range(f...  15.6 us
    reduce_scatter x1, waiting for transfers between devices, local(): lax.psum_scatter(contract_rows(down_whole, hidden).astype(jnp.bfloat16),...  12.9 us
  transfers between devices with their start and end apart: 12, of which 7 were waited for; matrix products, arithmetic and copies ran while one was open for 13% of the time, Pallas kernels for 0%

commit v1 on v0

--- a/solution.py
+++ b/solution.py
@@ -254,7 +254,7 @@
         jnp.concatenate([own_part, from_partner], axis=0),
         jnp.concatenate([from_partner, own_part], axis=0),
     )
-    down_whole = lax.all_gather(hidden_down, "sp", axis=1, tiled=True)
+    down_whole = jnp.concatenate(lax.all_gather(hidden_down, "sp"), axis=1)
     hidden_sum = lax.psum_scatter(
         contract_rows(down_whole, hidden).astype(jnp.bfloat16),
         "tp",

time: 632 us -> 610 us (0.965)
  waiting for transfers between devices: 272 us -> 233 us
  local copies, waits for them, and re-layouts: 26.2 us -> 40 us
    ppermute x2, waiting for transfers between devices: 85.5 us -> 39.2 us  [from_partner_2(): lax.ppermute(shard, axis, [(i, i ^ 1 << stride) for i in range(lax.axis_s...]
    all_to_all x1, waiting for transfers between devices: 75.9 us -> 90.7 us  [local(): lax.all_to_all(up_tiles, 'sp', split_axis=0, concat_axis=0, tiled=True)]
    reshape x0 -> x1, local copies, waits for them, and re-layouts: none -> 13.8 us  [local(): down_whole = jnp.concatenate(lax.all_gather(hidden_down, 'sp'), axis=1)]
  transfers between devices with their start and end apart: 12 -> 12, of which waited for: 7 -> 6; matrix products, arithmetic and copies ran while one was open for 13% -> 16% of each run, Pallas kernels for 0% -> 0%
where the time goes in v1:
time: 610 us; the launch traced here: 601 us
  waiting for transfers between devices  233 us (38%)
  blocking collectives  205 us (34%)
  matrix products  52.4 us (9%)
  local copies, waits for them, and re-layouts  40 us (7%)
  starting transfers between devices  33.3 us (5%)
  other arithmetic  22.8 us (4%)
  between operations  14.4 us (2%)
    all_gather x2, blocking collectives, prefix(): lax.all_gather(a.astype(kind), axis)  202 us
    all_to_all x1, waiting for transfers between devices, local(): lax.all_to_all(up_tiles, 'sp', split_axis=0, concat_axis=0, tiled=True)  90.7 us
    all_gather x1, waiting for transfers between devices, local(): down_whole = jnp.concatenate(lax.all_gather(hidden_down, 'sp'), axis=1)  57 us
    ppermute x2, waiting for transfers between devices, from_partner_2(): lax.ppermute(shard, axis, [(i, i ^ 1 << stride) for i in range(lax.axis_s...  39.2 us
    reduce_scatter x1, waiting for transfers between devices, local(): lax.psum_scatter(lax.dot_general(out_weight, normed, (((0,), (1,)), ((),...  36.7 us
    dot_general x3, matrix products, contract_rows(): lax.dot_general(left, right, (((0,), (0,)), ((), ())), preferred_element_...  20.3 us
    ppermute x2, starting transfers between devices, from_behind(): lax.ppermute(value, axis, [(source, source + steps) for source in range(f...  17.3 us
    reshape x1, local copies, waits for them, and re-layouts, local(): down_whole = jnp.concatenate(lax.all_gather(hidden_down, 'sp'), axis=1)  13.8 us
  transfers between devices with their start and end apart: 12, of which 6 were waited for; matrix products, arithmetic and copies ran while one was open for 16% of the time, Pallas kernels for 0%

profile of v1, /device:TPU:0, one launch (start us, length us, event | category | flops | bytes accessed | tf_op | source)
XLA Modules:
  0.0 600.7 jit_solution(12397288756124246646)
XLA Ops:
  8.2 4.9 collective-permute-start
  23.4 2.4 divide_multiply_fusion.1
  31.1 2.4 fusion.43
  34.7 2.8 tile.8
  37.5 6.0 all-to-all-start
  53.7 125.0 %all-gather.5 = bf16[16,4,4]{2,1,0:T(4,128)(2,1)S(1)} all-gather(bf16[1,4,4]{2,1,0:T(4,128)(2,1)S(1)} %get-tuple-element.151), channel_id=2, replica_groups=mesh['sp'=16,'tp'=2] {'sp'}, dimensions={0}, use_global_device_ids=true | all-gather | bytes 544 | tf_op jit(solution)/shard_map/all_gather | solution.py:24
  178.7 77.4 %all-gather.6 = bf16[16,4,4]{2,1,0:T(4,128)(2,1)S(1)} all-gather(bf16[1,4,4]{2,1,0:T(4,128)(2,1)S(1)} %get-tuple-element.150), channel_id=4, replica_groups=mesh['sp'=16,'tp'=2] {'sp'}, dimensions={0}, use_global_device_ids=true | all-gather | bytes 544 | tf_op jit(solution)/shard_map/all_gather | solution.py:24
  263.3 3.0 fusion.38
  266.3 2.9 fusion.32
  269.2 3.0 fusion.34
  280.2 2.5 psum.7
  282.6 7.0 %fusion.6 = bf16[2048,256]{0,1:T(8,128)(2,1)} fusion(bf16[2048,2048]{1,0:T(8,128)(2,1)} %param.28, f32[2048]{0:T(1024)S(1)} %copy-done.18, f32[256]{0:T(256)S(1)} %add_rsqrt_fusion.1, f32[256,2048]{1,0:T(8,128)S(1)} %copy.154, bf16[256,2048]{1,0:T(8,128)(2,1)S(1)} %copy-done.5), kind=kOutput, calls=%fused_computation.24 | convolution fusion | flops 2152726528 | bytes 12592128 | tf_op jit(solution)/shard_map/dot_general | solution.py:205
  291.0 36.7 %reduce-scatter.3.cloned.1.call-done = bf16[1024,256]{0,1:T(8,128)(2,1)} async-done(((bf16[2048,256]{0,1:T(8,128)(2,1)}), bf16[1024,256]{0,1:T(8,128)(2,1)}) %reduce-scatter.3.cloned.1.call-update) | async-done | bytes 524304 | tf_op jit(solution)/shard_map/reduce_scatter | solution.py:204
  330.5 2.8 tile.20
  333.4 6.9 %all-to-all-start.1 = ((bf16[16,128,1280]{2,1,0:T(8,128)(2,1)}), bf16[16,128,1280]{2,1,0:T(8,128)(2,1)}, u32[]{:S(2)}, u32[]{:S(2)}) async-start(bf16[16,128,1280]{2,1,0:T(8,128)(2,1)} %bitcast.264), calls=%async_computation.2 | async-start | bytes 10485760 | tf_op jit(solution)/shard_map/all_to_all | solution.py:232
  345.4 39.2 %collective-permute-done.1 = bf16[2048,256]{0,1:T(8,128)(2,1)S(1)} collective-permute-done((bf16[2048,256]{0,1:T(8,128)(2,1)S(1)}, bf16[2048,256]{0,1:T(8,128)(2,1)S(1)}, u32[]{:S(2)}, u32[]{:S(2)}) %collective-permute-start.1) | collective-permute-done | bytes 1048608 | tf_op jit(solution)/shard_map/ppermute | solution.py:44
  384.6 5.8 fusion.2
  390.3 90.7 %all-to-all-done.1 = bf16[16,128,1280]{2,1,0:T(8,128)(2,1)} async-done(((bf16[16,128,1280]{2,1,0:T(8,128)(2,1)}), bf16[16,128,1280]{2,1,0:T(8,128)(2,1)}, u32[]{:S(2)}, u32[]{:S(2)}) %all-to-all-start.1) | async-done | bytes 5242912 | tf_op jit(solution)/shard_map/all_to_all | solution.py:232
  481.0 6.7 %fusion.3 = bf16[1,1280,512]{1,2,0:T(8,128)(2,1)S(1)} fusion(bf16[2048,1280]{1,0:T(8,128)(2,1)} %bitcast.75, bf16[2048,256]{0,1:T(8,128)(2,1)} %copy-done.17, bf16[2048,256]{0,1:T(8,128)(2,1)} %copy-done.7, pred[]{:T(512)S(6)} %eq.5), kind=kOutput, calls=%fused_computation.12 | convolution fusion | flops 2694447104 | bytes 8650753 | tf_op jit(solution)/shard_map/dot_general | solution.py:78
  487.7 12.4 %collective-permute-start.2 = (bf16[2,1280,2]{1,2,0:T(2,128)(2,1)S(1)}, bf16[2,1280,2]{1,2,0:T(2,128)(2,1)S(1)}, u32[]{:S(2)}, u32[]{:S(2)}) collective-permute-start(bf16[2,1280,2]{1,2,0:T(2,128)(2,1)S(1)} %pad_maximum_fusion.4), channel_id=1, source_target_pairs={{0,4},{2,6},{4,8},{6,10},{8,12},{10,14},{12,16},{14,18},{16,20},{1... | collective-permute-start | bytes 30728 | tf_op jit(solution)/shard_map/ppermute | solution.py:18
  505.3 57.0 %all-gather.18.cloned.1.call-done = bf16[40960,128]{1,0:T(8,128)(2,1)} async-done(((bf16[2560,128]{1,0:T(8,128)(2,1)}), bf16[40960,128]{1,0:T(8,128)(2,1)}) %all-gather.18.cloned.1.call-update) | async-done | bytes 10485776 | tf_op jit(solution)/shard_map/all_gather | solution.py:257
  562.4 13.8 %copy.155 = bf16[2560,16,128]{0,2,1:T(8,128)(2,1)} copy(bf16[2560,16,128]{2,0,1:T(8,128)(2,1)} %bitcast.279) | data formatting | bytes 20971520 | tf_op jit(solution)/shard_map/reshape | solution.py:257
  576.2 7.9 %fusion.7 = bf16[2048,256]{0,1:T(8,128)(2,1)} fusion(bf16[2560,2048]{0,1:T(8,128)(2,1)} %bitcast.280, bf16[1280,256]{0,1:T(8,128)(2,1)S(1)} %collective-permute-done.3, bf16[1280,256]{0,1:T(8,128)(2,1)S(1)} %get-tuple-element.121, pred[]{:T(512)S(6)} %eq.5), kind=kOutput, calls=%fused_computation.25 | convolution fusion | flops 2690777088 | bytes 12845057 | tf_op jit(solution)/shard_map/dot_general | solution.py:78
  584.1 7.3 %reduce-scatter.5.cloned.1.call-done = bf16[1024,256]{0,1:T(8,128)(2,1)} async-done(((bf16[2048,256]{0,1:T(8,128)(2,1)}), bf16[1024,256]{0,1:T(8,128)(2,1)}) %reduce-scatter.5.cloned.1.call-update) | async-done | bytes 524304 | tf_op jit(solution)/shard_map/reduce_scatter | solution.py:258
  (164 shorter events, 59.9 us)
Async XLA Ops:
  6.5 10.0 %copy-start.8 = (bf16[256,1536]{1,0:T(8,128)(2,1)S(1)}, bf16[256,1536]{1,0:T(8,128)(2,1)}, u32[]{:S(2)}) copy-start(bf16[256,1536]{1,0:T(8,128)(2,1)} %param.21) | copy-start | bytes 2359300
  6.5 10.0 %copy-start.13 = (bf16[4,1536]{1,0:T(4,128)(2,1)S(1)}, bf16[4,1536]{1,0:T(4,128)(2,1)}, u32[]{:S(2)}) copy-start(bf16[4,1536]{1,0:T(4,128)(2,1)} %param.26) | copy-start | bytes 36868
  6.5 265.7 %all-gather.16.cloned.1.call-start = ((), (), s32[]{:S(2)}) async-start(), calls=%async_computation.8 | async-start | bytes 4456448 | tf_op jit(solution)/shard_map/all_gather | solution.py:24
  8.2 9.8 %collective-permute-start = (bf16[3,3584]{1,0:T(4,128)(2,1)S(1)}, bf16[3,3584]{1,0:T(4,128)(2,1)S(1)}, u32[]{:S(2)}, u32[]{:S(2)}) collective-permute-start(bf16[3,3584]{1,0:T(4,128)(2,1)S(1)} %pad_maximum_fusion.3), channel_id=1, source_target_pairs={{0,2},{2,4},{4,6},{6,8},{8,10},{10,12},{12,14},{14,16},{16,18},{18... | collective-permute-start | bytes 64520 | tf_op jit(solution)/shard_map/ppermute | solution.py:18
  27.7 244.5 %all-gather.14.cloned.1.call-start = ((), (), s32[]{:S(2)}) async-start(), calls=%async_computation.7 | async-start | bytes 4456448 | tf_op jit(solution)/shard_map/all_gather | solution.py:24
  37.5 293.0 %all-to-all-start = ((bf16[16,128,1280]{2,1,0:T(8,128)(2,1)}), bf16[16,128,1280]{2,1,0:T(8,128)(2,1)}, u32[]{:S(2)}, u32[]{:S(2)}) async-start(bf16[16,128,1280]{2,1,0:T(8,128)(2,1)} %bitcast.263), calls=%async_computation.1 | async-start | bytes 10485760 | tf_op jit(solution)/shard_map/all_to_all | solution.py:231
  43.5 4.9 copy-start.12
  43.5 8.5 %copy-start.16 = (f32[32]{0:T(128)S(1)}, f32[32]{0:T(128)}, u32[]{:S(2)}) copy-start(f32[32]{0:T(128)} %param.24) | copy-start | bytes 388
  43.5 284.2 %reduce-scatter.3.cloned.1.call-start = ((), (), s32[]{:S(2)}) async-start(), calls=%async_computation.4 | async-start | bytes 1572864 | tf_op jit(solution)/shard_map/reduce_scatter | solution.py:204
  47.3 4.8 copy-start.6
  279.4 3.3 copy-start.18
  289.6 40.7 %copy-start.9 = (bf16[128,2560]{1,0:T(8,128)(2,1)S(1)}, bf16[128,2560]{1,0:T(8,128)(2,1)}, u32[]{:S(2)}) copy-start(bf16[128,2560]{1,0:T(8,128)(2,1)} %param.31) | copy-start | bytes 1966084
  289.6 50.7 %all-gather.12.cloned.1.call-start = ((), (), s32[]{:S(2)}) async-start(), calls=%async_computation.5 | async-start | bytes 1572864 | tf_op jit(solution)/shard_map/all_gather | solution.py:213
  329.8 232.6 %all-gather.18.cloned.1.call-start = ((), (), s32[]{:S(2)}) async-start(), calls=%async_computation.9 | async-start | bytes 11141120 | tf_op jit(solution)/shard_map/all_gather | solution.py:257
  333.3 8.6 %copy-start.14 = (f32[2048]{0:T(1024)S(1)}, f32[2048]{0:T(1024)}, u32[]{:S(2)}) copy-start(f32[2048]{0:T(1024)} %param.29) | copy-start | bytes 24580
  333.4 147.7 %all-to-all-start.1 = ((bf16[16,128,1280]{2,1,0:T(8,128)(2,1)}), bf16[16,128,1280]{2,1,0:T(8,128)(2,1)}, u32[]{:S(2)}, u32[]{:S(2)}) async-start(bf16[16,128,1280]{2,1,0:T(8,128)(2,1)} %bitcast.264), calls=%async_computation.2 | async-start | bytes 10485760 | tf_op jit(solution)/shard_map/all_to_all | solution.py:232
  340.3 251.1 %reduce-scatter.5.cloned.1.call-start = ((), (), s32[]{:S(2)}) async-start(), calls=%async_computation.6 | async-start | bytes 1572864 | tf_op jit(solution)/shard_map/reduce_scatter | solution.py:258
  343.4 46.9 %copy-start.7 = (bf16[2048,256]{0,1:T(8,128)(2,1)}, bf16[2048,256]{0,1:T(8,128)(2,1)S(1)}, u32[]{:S(2)}) copy-start(bf16[2048,256]{0,1:T(8,128)(2,1)S(1)} %fusion.14) | copy-start | bytes 3145732
  343.5 41.1 %collective-permute-start.1 = (bf16[2048,256]{0,1:T(8,128)(2,1)S(1)}, bf16[2048,256]{0,1:T(8,128)(2,1)S(1)}, u32[]{:S(2)}, u32[]{:S(2)}) collective-permute-start(bf16[2048,256]{0,1:T(8,128)(2,1)S(1)} %fusion.14), channel_id=1, source_target_pairs={{0,2},{2,0},{4,6},{6,4},{8,10},{10,8},{12,14},{14,12},{16,18},{18,... | collective-permute-start | bytes 3145736 | tf_op jit(solution)/shard_map/ppermute | solution.py:44
  384.5 5.8 copy-start.17
  487.7 12.5 %copy-start.15 = (bf16[2,3,2560]{2,0,1:T(2,128)(2,1)S(1)}, bf16[2,3,2560]{2,0,1:T(2,128)(2,1)}, u32[]{:S(2)}) copy-start(bf16[2,3,2560]{2,0,1:T(2,128)(2,1)} %param.32) | copy-start | bytes 92164
  487.7 13.7 %collective-permute-start.2 = (bf16[2,1280,2]{1,2,0:T(2,128)(2,1)S(1)}, bf16[2,1280,2]{1,2,0:T(2,128)(2,1)S(1)}, u32[]{:S(2)}, u32[]{:S(2)}) collective-permute-start(bf16[2,1280,2]{1,2,0:T(2,128)(2,1)S(1)} %pad_maximum_fusion.4), channel_id=1, source_target_pairs={{0,4},{2,6},{4,8},{6,10},{8,12},{10,14},{12,16},{14,18},{16,20},{1... | collective-permute-start | bytes 30728 | tf_op jit(solution)/shard_map/ppermute | solution.py:18
  504.4 71.7 %collective-permute-start.3 = (bf16[1280,256]{0,1:T(8,128)(2,1)S(1)}, bf16[1280,256]{0,1:T(8,128)(2,1)S(1)}, u32[]{:S(2)}, u32[]{:S(2)}) collective-permute-start(bf16[1280,256]{0,1:T(8,128)(2,1)S(1)} %get-tuple-element.122), channel_id=1, source_target_pairs={{0,2},{2,0},{4,6},{6,4},{8,10},{10,8},{12,14},{14,12},{16,18},{18,... | collective-permute-start | bytes 1966088 | tf_op jit(solution)/shard_map/ppermute | solution.py:44
  576.2 15.2 %copy-start.2 = (bf16[1024,256]{0,1:T(8,128)(2,1)S(1)}, bf16[1024,256]{0,1:T(8,128)(2,1)}, u32[]{:S(2)}) copy-start(bf16[1024,256]{0,1:T(8,128)(2,1)} %add_convert_fusion.1) | copy-start | bytes 1572868
  (7 other events, 14.9 us)
Sparse Core Ops, SparseCore 0:
  27.9 156.5 all-gather.15
  187.3 74.8 all-gather.13
  289.8 37.9 reduce-scatter.2
  329.9 10.1 all-gather.11
  342.7 219.6 all-gather.17
  584.2 7.0 reduce-scatter.4
